TPU v7x, 32 devices: a whole 2x2x4 slice. The times are simulated.
32 devices in a mesh: fs: 16 (over z, y, x), tp: 2 (over core).
Axes of the slice: x: 2, y: 2, z: 4, core: 2. Of those that a mesh axis runs over, the one named last changes fastest.
Arguments:
- fwd_tokens: bfloat16 [2048, 2048], P('fs'), may hold values from -6 to 6
- back_tokens: bfloat16 [2048, 2048], P('fs'), may hold values from -6 to 6
- out_grad: bfloat16 [2048, 2048], P('fs'), may hold values from -6 to 6
- norm_gain: float32 [2048], replicated, may hold values from 0.1 to 1.9
- gate_weight: bfloat16 [2048, 2816], P('fs', 'tp'), may hold values from -0.125 to 0.125
- up_weight: bfloat16 [2048, 2816], P('fs', 'tp'), may hold values from -0.125 to 0.125
- down_weight: bfloat16 [2048, 2816], P('fs', 'tp'), may hold values from -0.109375 to 0.109375
- gate_grad_sum: float32 [2048, 2816], P('fs', 'tp'), may hold values from -96 to 96
Outputs:
- fwd_out: bfloat16 [2048, 2048], P('fs')
- back_grad: bfloat16 [2048, 2048], P('fs')
- gate_grad_out: float32 [2048, 2816], P('fs', 'tp')
All inputs are finite; a program needn't handle non-finite values.
Results may differ from a plain program's by a relative error of at most 0.014.
Values may be sent and summed in bfloat16 or wider, within the bound.
A program may use at most 64 MiB of HBM per device.

v0:
```python
import jax
import jax.numpy as jnp
from jax import lax
from jax.sharding import PartitionSpec as P

norm_eps = 0.25


def normalize(tokens, norm_gain):
    values = tokens.astype(jnp.float32)
    factor = lax.rsqrt(jnp.mean(values * values, axis=-1, keepdims=True) + norm_eps)
    return (values, factor, (values * factor * norm_gain).astype(jnp.bfloat16))


def shards(
    fwd_tokens, back_tokens, out_grad, norm_gain, gate_weight, up_weight, down_weight, gate_grad_sum
):
    fwd_normed = normalize(fwd_tokens, norm_gain)[2]
    columns = fwd_normed
    gate_pre = jnp.dot(
        columns,
        lax.all_gather(gate_weight, "fs", axis=0, tiled=True),
        preferred_element_type=jnp.float32,
    )
    up_pre = jnp.dot(
        columns,
        lax.all_gather(up_weight, "fs", axis=0, tiled=True),
        preferred_element_type=jnp.float32,
    )
    hidden = (gate_pre * jax.nn.sigmoid(gate_pre) * up_pre).astype(jnp.bfloat16)
    partial_value = jnp.dot(
        hidden,
        lax.all_gather(down_weight, "fs", axis=0, tiled=True).T,
        preferred_element_type=jnp.float32,
    )
    summed = lax.psum(partial_value.astype(jnp.bfloat16), "tp").astype(jnp.float32)
    fwd_out = (0.5 * summed).astype(jnp.bfloat16)
    gate_whole = lax.all_gather(gate_weight, "fs", axis=0, tiled=True)
    up_whole = lax.all_gather(up_weight, "fs", axis=0, tiled=True)
    down_whole = lax.all_gather(down_weight, "fs", axis=0, tiled=True)
    values, factor, back_normed = normalize(back_tokens, norm_gain)
    gate_pre = jnp.dot(back_normed, gate_whole, preferred_element_type=jnp.float32)
    up_pre = jnp.dot(back_normed, up_whole, preferred_element_type=jnp.float32)
    sigmoid_gate = jax.nn.sigmoid(gate_pre)
    back_hidden = 0.5 * jnp.dot(out_grad, down_whole, preferred_element_type=jnp.float32)
    gate_diff = (
        back_hidden * up_pre * sigmoid_gate * (1.0 + gate_pre * (1.0 - sigmoid_gate))
    ).astype(jnp.bfloat16)
    up_diff = (back_hidden * gate_pre * sigmoid_gate).astype(jnp.bfloat16)
    columns = back_normed
    gate_grad_out = gate_grad_sum + lax.psum_scatter(
        jnp.dot(columns.T, gate_diff, preferred_element_type=jnp.float32),
        "fs",
        scatter_dimension=0,
        tiled=True,
    )
    partial_diff = jnp.dot(gate_diff, gate_whole.T, preferred_element_type=jnp.float32)
    partial_diff = partial_diff + jnp.dot(up_diff, up_whole.T, preferred_element_type=jnp.float32)
    normed_diff = lax.psum(partial_diff.astype(jnp.bfloat16), "tp").astype(jnp.float32)
    scaled = normed_diff * norm_gain
    cubed = factor * factor * factor
    back_grad = (
        factor * scaled - values * cubed * jnp.mean(scaled * values, axis=-1, keepdims=True)
    ).astype(jnp.bfloat16)
    back_grad, gate_grad_out = (back_grad, gate_grad_out)
    return (fwd_out, back_grad, gate_grad_out)


def solution(mesh):
    in_specs = (
        P("fs", None),
        P("fs", None),
        P("fs", None),
        P(),
        P("fs", "tp"),
        P("fs", "tp"),
        P("fs", "tp"),
        P("fs", "tp"),
    )
    out_specs = (P("fs", None), P("fs", None), P("fs", "tp"))
    return jax.shard_map(shards, mesh=mesh, in_specs=in_specs, out_specs=out_specs, check_vma=False)
```

profile of v0, /device:TPU:10, one launch (start us, length us, event | category | flops | bytes accessed | tf_op | source)
XLA Modules:
  0.0 574.4 jit_solution(14257053554453294559)
XLA Ops:
  7.2 0.0 copy-start
  7.2 0.0 all-gather.8.cloned.1.call-start
  7.2 0.7 all-gather.8.cloned.1.call-update
  7.9 0.0 all-gather.4.cloned.1.call-start
  8.0 0.7 all-gather.4.cloned.1.call-update
  8.7 0.0 all-gather.6.cloned.1.call-start
  8.7 0.7 all-gather.6.cloned.1.call-update
  9.4 0.0 all-reduce.3.cloned.1.call-start
  9.5 1.2 fusion.5
  10.7 1.2 fusion.8
  11.9 0.0 copy-start.2
  12.0 88.5 %all-gather.8.cloned.1.call-done = bf16[2048,1408]{1,0:T(8,128)(2,1)} async-done(((bf16[128,1408]{1,0:T(8,128)(2,1)}), bf16[2048,1408]{1,0:T(8,128)(2,1)}) %all-gather.8.cloned.1.call-update) | async-done | bytes 5767184 | tf_op jit(solution)/shard_map/all_gather | solution.py:33
  100.5 4.5 convolution_multiply_fusion.1
  105.0 85.6 %all-gather.4.cloned.1.call-done = bf16[2048,1408]{1,0:T(8,128)(2,1)} async-done(((bf16[128,1408]{1,0:T(8,128)(2,1)}), bf16[2048,1408]{1,0:T(8,128)(2,1)}) %all-gather.4.cloned.1.call-update) | async-done | bytes 5767184 | tf_op jit(solution)/shard_map/all_gather | solution.py:22
  190.6 4.7 fusion.19
  195.3 1.9 fusion.25
  197.3 83.5 %all-gather.6.cloned.1.call-done = bf16[2048,1408]{1,0:T(8,128)(2,1)} async-done(((bf16[128,1408]{1,0:T(8,128)(2,1)}), bf16[2048,1408]{1,0:T(8,128)(2,1)}) %all-gather.6.cloned.1.call-update) | async-done | bytes 5767184 | tf_op jit(solution)/shard_map/all_gather | solution.py:27
  280.8 8.3 %convolution_convert_fusion = bf16[128,2048]{1,0:T(8,128)(2,1)} fusion(bf16[2048,1408]{1,0:T(8,128)(2,1)} %all-gather.8.cloned.1.call-done, bf16[2048,1408]{1,0:T(8,128)(2,1)} %all-gather.6.cloned.1.call-done, f32[128,1408]{1,0:T(8,128)} %fusion.19, bf16[128,2048]{1,0:T(8,128)(2,1)S(1)} %copy-done.3, f32[2048]{0:T(1024)S(1)} %copy-done.7, ...), kind=kOutput, calls=%fused_computation.9 | convolution fusion | flops 1478787072 | bytes 13312512 | tf_op jit(solution)/shard_map/dot_general | solution.py:31
  289.1 4.3 fusion.2
  293.4 2.0 fusion.28
  295.4 0.0 copy-done.5
  295.4 0.2 copy-done.6
  295.6 2.8 fusion.3
  298.4 0.0 all-reduce.3.cloned.1.call-update
  298.4 0.0 reduce-scatter.2.cloned.1.call-start
  298.4 6.1 %fusion.23 = f32[2048,1408]{1,0:T(8,128)} fusion(bf16[128,1408]{1,0:T(8,128)(2,1)S(1)} %fusion.2, bf16[128,2048]{1,0:T(8,128)(2,1)S(1)} %copy-done.2, f32[128]{0:T(128)S(1)} %get-tuple-element.6, f32[2048]{0:T(1024)S(1)} %copy-done.7), kind=kOutput, calls=%fused_computation.39 | convolution fusion | flops 739246080 | bytes 12427776 | tf_op jit(solution)/shard_map/dot_general | solution.py:52
  304.5 0.0 reduce-scatter.2.cloned.1.call-update
  304.6 12.6 %all-reduce.3.cloned.1.call-done = (bf16[128,2048]{1,0:T(8,128)(2,1)}, bf16[128,2048]{1,0:T(8,128)(2,1)}) async-done(((bf16[128,2048]{1,0:T(8,128)(2,1)}, bf16[128,2048]{1,0:T(8,128)(2,1)}), (bf16[128,2048]{1,0:T(8,128)(2,1)}, bf16[128,2048]{1,0:T(8,128)(2,1)})) %all-reduce.3.cloned.1.call-update) | async-done | bytes 1048592 | tf_op jit(solution)/shard_map/psum | solution.py:36
  317.1 1.3 fusion.14
  318.4 2.7 fusion.13
  321.1 244.7 %reduce-scatter.2.cloned.1.call-done = f32[128,1408]{1,0:T(8,128)} async-done(((f32[2048,1408]{1,0:T(8,128)}), f32[128,1408]{1,0:T(8,128)}) %reduce-scatter.2.cloned.1.call-update) | async-done | bytes 720912 | tf_op jit(solution)/shard_map/reduce_scatter | solution.py:51
  565.8 2.0 add.46
  (22 shorter events, 0.1 us)
Async XLA Ops:
  7.2 93.3 %copy-start = (bf16[128,2048]{1,0:T(8,128)(2,1)S(1)}, bf16[128,2048]{1,0:T(8,128)(2,1)}, u32[]{:S(2)}) copy-start(bf16[128,2048]{1,0:T(8,128)(2,1)} %param.10) | copy-start | bytes 1572868
  7.2 183.5 %copy-start.3 = (bf16[128,2048]{1,0:T(8,128)(2,1)S(1)}, bf16[128,2048]{1,0:T(8,128)(2,1)}, u32[]{:S(2)}) copy-start(bf16[128,2048]{1,0:T(8,128)(2,1)} %param.8) | copy-start | bytes 1572868
  7.2 183.4 %copy-start.7 = (f32[2048]{0:T(1024)S(1)}, f32[2048]{0:T(1024)}, u32[]{:S(2)}) copy-start(f32[2048]{0:T(1024)} %param.11) | copy-start | bytes 24580
  7.2 93.3 %all-gather.8.cloned.1.call-start = ((), (), s32[]{:S(2)}) async-start(), calls=%async_computation.3 | async-start | bytes 6127616 | tf_op jit(solution)/shard_map/all_gather | solution.py:33
  7.9 182.7 %all-gather.4.cloned.1.call-start = ((), (), s32[]{:S(2)}) async-start(), calls=%async_computation.1 | async-start | bytes 6127616 | tf_op jit(solution)/shard_map/all_gather | solution.py:22
  8.7 272.1 %all-gather.6.cloned.1.call-start = ((), (), s32[]{:S(2)}) async-start(), calls=%async_computation.2 | async-start | bytes 6127616 | tf_op jit(solution)/shard_map/all_gather | solution.py:27
  9.4 307.7 %all-reduce.3.cloned.1.call-start = ((), (), s32[]{:S(2)}) async-start(), calls=%async_computation.5 | async-start | bytes 2097152 | tf_op jit(solution)/shard_map/psum | solution.py:36
  11.9 183.4 %copy-start.2 = (bf16[128,2048]{1,0:T(8,128)(2,1)S(1)}, bf16[128,2048]{1,0:T(8,128)(2,1)}, u32[]{:S(2)}) copy-start(bf16[128,2048]{1,0:T(8,128)(2,1)} %param.9) | copy-start | bytes 1572868
  190.6 4.7 copy-start.1
  280.8 12.6 %slice-start = ((s8[5767168]{0:T(1024)(128)(4,1)}), s8[1572864]{0:T(1024)(128)(4,1)S(1)}, s32[]{:S(2)}) async-start(s8[5767168]{0:T(1024)(128)(4,1)} %bitcast.11), calls=%async_computation.6 | async-start | bytes 3145728
  289.1 4.3 slice-start.1
  289.1 6.3 %copy-start.8 = (bf16[2048,1408]{1,0:T(8,128)(2,1)S(1)}, bf16[2048,1408]{1,0:T(8,128)(2,1)}, u32[]{:S(2)}) copy-start(bf16[2048,1408]{1,0:T(8,128)(2,1)} %all-gather.6.cloned.1.call-done) | copy-start | bytes 17301508
  293.4 2.0 copy-start.5
  293.4 2.2 copy-start.6
  298.4 267.4 %reduce-scatter.2.cloned.1.call-start = ((), (), s32[]{:S(2)}) async-start(), calls=%async_computation.4 | async-start | bytes 12255232 | tf_op jit(solution)/shard_map/reduce_scatter | solution.py:51
  304.5 261.3 %copy-start.4 = (f32[128,1408]{1,0:T(8,128)S(1)}, f32[128,1408]{1,0:T(8,128)}, u32[]{:S(2)}) copy-start(f32[128,1408]{1,0:T(8,128)} %param.15) | copy-start | bytes 2162692
Sparse Core Ops, SparseCore 0:
  10.7 89.7 all-gather.7
  103.2 87.4 all-gather.3
  193.3 87.4 all-gather.5
  298.5 18.5 all-reduce.2
  319.3 246.4 reduce-scatter.1
where the time goes:
time: 575 us; the launch traced here: 574 us
  waiting for transfers between devices  517 us (90%)
  matrix products  34.5 us (6%)
  between operations  13.9 us (2%)
  other arithmetic  8.52 us (1%)
    reduce_scatter x1, waiting for transfers between devices, shards(): lax.psum_scatter(jnp.dot(columns.T, gate_diff, preferred_element_type=jnp...  245 us
    all_gather x1, waiting for transfers between devices, shards(): lax.all_gather(down_weight, 'fs', axis=0, tiled=True)  88.5 us
    all_gather x1, waiting for transfers between devices, shards(): lax.all_gather(gate_weight, 'fs', axis=0, tiled=True)  85.6 us
    all_gather x1, waiting for transfers between devices, shards(): lax.all_gather(up_weight, 'fs', axis=0, tiled=True)  83.5 us
    psum x1, waiting for transfers between devices, shards(): lax.psum(partial_value.astype(jnp.bfloat16), 'tp').astype(jnp.float32)  12.6 us
  transfers between devices with their start and end apart: 5, of which 5 were waited for; matrix products, arithmetic and copies ran while one was open for 4% of the time, Pallas kernels for 0%

commit v1 on v0

--- a/solution.py
+++ b/solution.py
@@ -1,6 +1,10 @@
+import functools
+
 import jax
 import jax.numpy as jnp
 from jax import lax
+from jax.experimental import pallas as pl
+from jax.experimental.pallas import tpu as pltpu
 from jax.sharding import PartitionSpec as P
 
 norm_eps = 0.25
@@ -66,6 +70,408 @@
     return (fwd_out, back_grad, gate_grad_out)
 
 
+MESH = pl.DeviceIdType.MESH
+
+
+def wide_dot(a, b):
+    return lax.dot_general(a, b, (((1,), (1,)), ((), ())), preferred_element_type=jnp.float32)
+
+
+def layer_kernel(
+    planes, plane, fwd_ref, back_ref, grad_ref, tokens_ref, gain_ref, gate_ref, up_ref, down_ref, sum_ref,
+    fwd_out, back_out, sum_out,
+    toks, weights, fwd_gate, fwd_up, back_gate, back_up, hidden, gate_diff, up_diff,
+    part, crossed, joined, gathered, grad_send, grad_recv, grad_cols,
+    stage_sem, weight_sem, up_sem, down_sem, tok_send, tok_recv, relay_send, relay_recv,
+    grad_send_sem, grad_recv_sem, cross_sem, join_send, join_recv, last_sem,
+):
+    n_fs = planes * plane
+    fs, core = lax.axis_index("fs"), lax.axis_index("tp")
+    level, place = fs // plane, fs % plane
+    sibling = (fs, 1 - core)
+    rows = weights.shape[1]
+    depth = gate_ref.shape[1]
+    half = fwd_ref.shape[0] // 2
+    slab = half * plane
+    width = fwd_ref.shape[1]
+
+    barrier = pltpu.get_barrier_semaphore()
+    for step in range(1, n_fs):
+        pl.semaphore_signal(barrier, inc=1, device_id=((fs + step) % n_fs, core), device_id_type=MESH)
+    pl.semaphore_signal(barrier, inc=1, device_id=sibling, device_id_type=MESH)
+    pl.semaphore_wait(barrier, n_fs)
+
+    def remote(src, dst, send, recv, device):
+        return pltpu.make_async_remote_copy(
+            src_ref=src, dst_ref=dst, send_sem=send, recv_sem=recv, device_id=device, device_id_type=MESH
+        )
+
+    own = (gate_ref, up_ref, down_ref)
+
+    def own_block(w, q):
+        return own[w].at[pl.ds(pl.multiple_of(q * rows, rows), rows), :]
+
+    def block(w, src):
+        return weights.at[w, :, pl.ds(pl.multiple_of(src * depth, depth), depth)]
+
+    def staged(w, step):
+        q = (place + step) % plane
+        return remote(own_block(w, q), block(w, fs), stage_sem.at[w, step], weight_sem.at[w, fs], (level * plane + q, core))
+
+    def arrived(w, src):
+        remote(block(w, src), block(w, src), stage_sem.at[w, 0], weight_sem.at[w, src], sibling).wait_recv()
+
+    def hop(w, src, source, step):
+        sem = up_sem if step > 0 else down_sem
+        return remote(source, block(w, src), sem.at[w, src], weight_sem.at[w, src], ((fs + step * plane + n_fs) % n_fs, core))
+
+    can = {1: level < planes - 1, -1: level > 0}
+
+    def send_on(w, src, source, step):
+        @pl.when(can[step])
+        def _():
+            hop(w, src, source, step).start()
+
+    token_refs = (back_ref, fwd_ref, grad_ref)
+
+    def tok_block(a, h, q):
+        return toks.at[a, h, pl.ds(pl.multiple_of(q * half, half), half), :]
+
+    def tok_copy(a, step):
+        q = (place + step) % plane
+        return remote(
+            token_refs[a].at[pl.ds(pl.multiple_of(core * half, half), half), :],
+            tok_block(a, core, place), tok_send.at[a, step], tok_recv.at[a, place], (level * plane + q, core),
+        )
+
+    def tok_arrived(a, q):
+        remote(tok_block(a, core, q), tok_block(a, core, q), tok_send.at[a, 0], tok_recv.at[a, q], sibling).wait_recv()
+
+    def relay(a, q):
+        return remote(tok_block(a, core, q), tok_block(a, core, q), relay_send.at[a, q], relay_recv.at[a, q], sibling)
+
+    def relayed(a, q):
+        remote(tok_block(a, 1 - core, q), tok_block(a, 1 - core, q), relay_send.at[a, q], relay_recv.at[a, q], sibling).wait_recv()
+
+    for w in range(3):
+        for step in range(1, plane):
+            staged(w, step).start()
+        for step in (1, -1):
+            send_on(w, fs, own_block(w, place), step)
+    for a in range(3):
+        for step in range(1, plane):
+            tok_copy(a, step).start()
+    for w in range(3):
+        weights[w, :, pl.ds(pl.multiple_of(fs * depth, depth), depth)] = own[w][pl.ds(pl.multiple_of(place * rows, rows), rows), :]
+    for a in range(3):
+        for h in range(2):
+            toks[a, h, pl.ds(pl.multiple_of(place * half, half), half), :] = token_refs[a][pl.ds(h * half, half), :]
+
+    def group(w, d):
+        if d == 0:
+            for step in range(1, plane):
+                src = level * plane + (place + step) % plane
+                arrived(w, src)
+                for way in (1, -1):
+                    send_on(w, src, block(w, src), way)
+            return
+        for way in (1, -1):
+            other = level - way * d
+
+            @pl.when(jnp.logical_and(other >= 0, other < planes))
+            def _():
+                @pl.loop(0, plane)
+                def _(q):
+                    src = other * plane + q
+                    arrived(w, src)
+                    send_on(w, src, block(w, src), way)
+
+    def relays(a):
+        for step in range(1, plane):
+            q = (place + step) % plane
+            tok_arrived(a, q)
+            relay(a, q).start()
+
+    def relays_in(a):
+        for step in range(1, plane):
+            relayed(a, (place + step) % plane)
+
+    def project(a, w, out):
+        @pl.loop(0, 2)
+        def _(h):
+            out[h] = wide_dot(toks[a, h], weights[w])
+
+    for wave in range(planes):
+        for w in range(3):
+            d = wave - w
+            if 0 <= d < planes:
+                group(w, d)
+    relays(0)
+    relays(1)
+    relays_in(0)
+    project(0, 0, back_gate)
+    relays_in(1)
+    project(1, 0, fwd_gate)
+    relays(2)
+    for w in range(1, 3):
+        if 0 <= planes - w < planes:
+            group(w, planes - w)
+    relays_in(2)
+    project(0, 1, back_up)
+    project(1, 1, fwd_up)
+
+    piece = 64
+
+    @pl.loop(0, 2)
+    def _(h):
+        @pl.loop(0, slab // piece)
+        def _(r):
+            at = pl.ds(pl.multiple_of(r * piece, piece), piece)
+            gate = fwd_gate[h, at, :]
+            hidden[h, at, :] = (gate * jax.nn.sigmoid(gate) * fwd_up[h, at, :]).astype(jnp.bfloat16)
+            gate = back_gate[h, at, :]
+            s = jax.nn.sigmoid(gate)
+            back_gate[h, at, :] = gate * s
+            back_up[h, at, :] = back_up[h, at, :] * s * (1.0 + gate * (1.0 - s))
+
+    for w in range(2, 3):
+        group(w, planes - 1)
+
+    @pl.loop(0, 2)
+    def _(h):
+        back = 0.5 * wide_dot(toks[2, h], weights[2])
+        fwd_gate[h] = back
+        gate_diff[pl.ds(pl.multiple_of(h * slab, slab), slab), :] = (back * back_up[h]).astype(jnp.bfloat16)
+        up_diff[pl.ds(pl.multiple_of(h * slab, slab), slab), :] = (back * back_gate[h]).astype(jnp.bfloat16)
+
+    def grad_copy(step):
+        to = (fs + step) % n_fs
+        return remote(grad_send.at[to], grad_recv.at[fs], grad_send_sem.at[to], grad_recv_sem.at[fs], (to, core))
+
+    diff_turned = gate_diff[...].T
+
+    for step in range(planes):
+        there = (level + step + 1) % planes
+        cols = pl.ds(pl.multiple_of(there * plane * depth, plane * depth), plane * depth)
+        product = jnp.dot(diff_turned[:, :slab], toks[0, 0, :, cols], preferred_element_type=jnp.float32)
+        product = product + jnp.dot(diff_turned[:, slab:], toks[0, 1, :, cols], preferred_element_type=jnp.float32)
+        product = product.astype(jnp.bfloat16)
+        for q in range(plane):
+            grad_send[there * plane + q] = product[:, q * depth : (q + 1) * depth]
+        for q in range(plane):
+            to = there * plane + q
+
+            @pl.when(to != fs)
+            def _():
+                remote(grad_send.at[to], grad_recv.at[fs], grad_send_sem.at[to], grad_recv_sem.at[fs], (to, core)).start()
+
+    grad_recv[fs] = grad_send[fs]
+
+    def cross(k):
+        return remote(part.at[k, 1 - core], crossed.at[k], cross_sem.at[k, 0], cross_sem.at[k, 1], sibling)
+
+    def join(k, step):
+        q = (place + step) % plane
+        return remote(joined.at[k, q], gathered.at[k, place], join_send.at[k, step], join_recv.at[k, place], (level * plane + q, core))
+
+    strip = 512
+
+    def partial(k, h):
+        rows_at = pl.ds(pl.multiple_of(h * slab, slab), slab)
+
+        @pl.loop(0, width // strip)
+        def _(t):
+            at = pl.ds(pl.multiple_of(t * strip, strip), strip)
+            if k == 0:
+                value = jnp.dot(hidden[h], weights[2, :, at], preferred_element_type=jnp.float32)
+            else:
+                value = jnp.dot(gate_diff[rows_at, :], weights[0, :, at], preferred_element_type=jnp.float32)
+                value = value + jnp.dot(up_diff[rows_at, :], weights[1, :, at], preferred_element_type=jnp.float32)
+            part[k, h, :, at] = value.astype(jnp.bfloat16)
+
+    for k in range(2):
+        partial(k, 1 - core)
+        cross(k).start()
+    for k in range(2):
+        partial(k, core)
+    for k in range(2):
+        cross(k).wait_recv()
+        for step in range(plane):
+            q = (place + step + 1) % plane
+            at = pl.ds(pl.multiple_of(q * half, half), half)
+            total = part[k, core, at, :].astype(jnp.float32) + crossed[k, at, :].astype(jnp.float32)
+            joined[k, q] = total.astype(jnp.bfloat16)
+            if step < plane - 1:
+                join(k, step + 1).start()
+    for k in range(2):
+        gathered[k, place] = joined[k, place]
+
+    mine = pl.ds(pl.multiple_of(core * half, half), half)
+
+    def last(k):
+        out = (fwd_out, back_out)[k]
+        return remote(out.at[mine, :], out.at[mine, :], last_sem.at[k, 0], last_sem.at[k, 1], sibling)
+
+    def joined_in(k):
+        for step in range(1, plane):
+            q = (place + step) % plane
+            remote(joined.at[k, q], gathered.at[k, q], join_send.at[k, 0], join_recv.at[k, q], sibling).wait_recv()
+
+    def total_of(k, at):
+        value = gathered[k, 0, at, :].astype(jnp.float32)
+        for q in range(1, plane):
+            value = value + gathered[k, q, at, :].astype(jnp.float32)
+        return value
+
+    small = 16
+    joined_in(0)
+    for r in range(half // small):
+        at = pl.ds(r * small, small)
+        fwd_out[pl.ds(pl.multiple_of(core * half + r * small, small), small), :] = (0.5 * total_of(0, at)).astype(jnp.bfloat16)
+    joined_in(1)
+    for r in range(half // small):
+        at = pl.ds(r * small, small)
+        there = pl.ds(pl.multiple_of(core * half + r * small, small), small)
+        values = tokens_ref[there, :].astype(jnp.float32)
+        factor = lax.rsqrt(jnp.mean(values * values, axis=-1, keepdims=True) + norm_eps)
+        scaled = total_of(1, at) * gain_ref[...]
+        cubed = factor * factor * factor
+        back_out[there, :] = (
+            factor * scaled - values * cubed * jnp.mean(scaled * values, axis=-1, keepdims=True)
+        ).astype(jnp.bfloat16)
+    for k in range(2):
+        last(k).start()
+
+    for step in range(1, n_fs):
+        src = (fs + step) % n_fs
+        remote(grad_send.at[src], grad_recv.at[src], grad_send_sem.at[src], grad_recv_sem.at[src], sibling).wait_recv()
+    for q in range(plane):
+        total = grad_recv[q].astype(jnp.float32)
+        for z in range(1, planes):
+            total = total + grad_recv[z * plane + q].astype(jnp.float32)
+        grad_cols[q * rows : (q + 1) * rows, :] = total
+
+    @pl.loop(0, grad_cols.shape[0] // 128)
+    def _(t):
+        at = pl.ds(pl.multiple_of(t * 128, 128), 128)
+        sum_out[:, at] = sum_ref[:, at] + grad_cols[at, :].T
+
+    for w in range(3):
+        for step in range(1, plane):
+            staged(w, step).wait_send()
+        for way in (1, -1):
+            for d in range(planes - 1):
+                other = level - way * d
+
+                @pl.when(jnp.logical_and(can[way], jnp.logical_and(other >= 0, other < planes)))
+                def _():
+                    @pl.loop(0, plane)
+                    def _(q):
+                        src = other * plane + q
+                        hop(w, src, block(w, src), way).wait_send()
+
+    for a in range(3):
+        for step in range(1, plane):
+            tok_copy(a, step).wait_send()
+            relay(a, (place + step) % plane).wait_send()
+    for step in range(1, n_fs):
+        grad_copy(step).wait_send()
+    for k in range(2):
+        cross(k).wait_send()
+        for step in range(1, plane):
+            join(k, step).wait_send()
+        last(k).wait()
+
+
+def fused_shards(
+    planes, plane, fwd_tokens, back_tokens, out_grad, norm_gain, gate_weight, up_weight, down_weight, gate_grad_sum
+):
+    tokens, width = fwd_tokens.shape
+    depth, cols = gate_weight.shape
+    rows = cols // plane
+    half = tokens // 2
+    slab = half * plane
+    n_fs = planes * plane
+    fwd_normed = normalize(fwd_tokens, norm_gain)[2]
+    back_normed = normalize(back_tokens, norm_gain)[2]
+    narrow, full = jnp.bfloat16, jnp.float32
+    dma = pltpu.SemaphoreType.DMA
+    vmem = pl.BlockSpec(memory_space=pltpu.VMEM)
+    return pl.pallas_call(
+        functools.partial(layer_kernel, planes, plane),
+        out_shape=(
+            jax.ShapeDtypeStruct((tokens, width), narrow),
+            jax.ShapeDtypeStruct((tokens, width), narrow),
+            jax.ShapeDtypeStruct((depth, cols), full),
+        ),
+        in_specs=[vmem] * 9,
+        out_specs=(vmem,) * 3,
+        scratch_shapes=[
+            pltpu.VMEM((3, 2, slab, width), narrow),
+            pltpu.VMEM((3, rows, width), narrow),
+            pltpu.VMEM((2, slab, rows), full),
+            pltpu.VMEM((2, slab, rows), full),
+            pltpu.VMEM((2, slab, rows), full),
+            pltpu.VMEM((2, slab, rows), full),
+            pltpu.VMEM((2, slab, rows), narrow),
+            pltpu.VMEM((2 * slab, rows), narrow),
+            pltpu.VMEM((2 * slab, rows), narrow),
+            pltpu.VMEM((2, 2, slab, width), narrow),
+            pltpu.VMEM((2, slab, width), narrow),
+            pltpu.VMEM((2, plane, half, width), narrow),
+            pltpu.VMEM((2, plane, half, width), narrow),
+            pltpu.VMEM((n_fs, rows, depth), narrow),
+            pltpu.VMEM((n_fs, rows, depth), narrow),
+            pltpu.VMEM((cols, depth), full),
+            dma((3, plane)),
+            dma((3, n_fs)),
+            dma((3, n_fs)),
+            dma((3, n_fs)),
+            dma((3, plane)),
+            dma((3, plane)),
+            dma((3, plane)),
+            dma((3, plane)),
+            dma((n_fs,)),
+            dma((n_fs,)),
+            dma((2, 2)),
+            dma((2, plane)),
+            dma((2, plane)),
+            dma((2, 2)),
+        ],
+        compiler_params=pltpu.CompilerParams(
+            collective_id=0, has_side_effects=True, vmem_limit_bytes=56 * 2**20
+        ),
+    )(
+        fwd_normed, back_normed, out_grad, back_tokens, norm_gain.reshape(1, width),
+        gate_weight.T, up_weight.T, down_weight.T, gate_grad_sum,
+    )
+
+
+def square_side(count):
+    side = 1
+    while side * side * 4 <= count:
+        side *= 2
+    return side
+
+
+def body_for(mesh):
+    n_fs, plane = mesh.shape["fs"], square_side(mesh.shape["fs"])
+
+    def body(*args):
+        tokens, width = args[0].shape
+        depth, cols = args[4].shape
+        fits = (
+            mesh.shape["tp"] == 2 and n_fs % plane == 0 and n_fs // plane >= 3 and plane >= 2
+            and depth == 128 and cols % (plane * 16) == 0 and cols % 128 == 0
+            and tokens % 128 == 0 and width % 512 == 0
+        )
+        if not fits:
+            return shards(*args)
+        return fused_shards(n_fs // plane, plane, *args)
+
+    return body
+
+
 def solution(mesh):
     in_specs = (
         P("fs", None),
@@ -78,4 +484,4 @@
         P("fs", "tp"),
     )
     out_specs = (P("fs", None), P("fs", None), P("fs", "tp"))
-    return jax.shard_map(shards, mesh=mesh, in_specs=in_specs, out_specs=out_specs, check_vma=False)
+    return jax.shard_map(body_for(mesh), mesh=mesh, in_specs=in_specs, out_specs=out_specs, check_vma=False)

time: 575 us -> 144 us (0.25)
  the two profiles are of different devices: /device:TPU:10 before, /device:TPU:0 now
where the time goes in v1:
time: 144 us; the launch traced here: 143 us
  Pallas kernels  132 us (92%)
  local copies, waits for them, and re-layouts  7.84 us (5%)
  other arithmetic  2.75 us (2%)
    pallas_call x1, Pallas kernels, fused_shards(): pl.pallas_call(functools.partial(layer_kernel, planes, plane), out_shape=...  132 us
    unnamed x22, local copies, waits for them, and re-layouts  7.84 us

profile of v1, /device:TPU:0, one launch (start us, length us, event | category | flops | bytes accessed | tf_op | source)
XLA Modules:
  0.0 143.2 jit_solution(13423913191677819882)
XLA Ops:
  0.6 0.0 copy-start
  0.6 1.3 fusion
  1.9 0.0 copy-done
  1.9 0.0 copy-start.4
  1.9 0.2 fusion.3
  2.1 0.8 copy-done.4
  2.9 0.0 copy-start.5
  2.9 0.9 copy.11
  3.8 0.1 copy-done.5
  3.9 0.0 copy-start.6
  3.9 0.9 copy.12
  4.8 0.0 copy-start.1
  4.8 0.1 copy-done.6
  4.9 0.0 copy-start.7
  4.9 0.9 copy.13
  5.8 0.1 copy-done.1
  5.9 0.0 copy-done.7
  5.9 1.3 fusion.5
  7.1 131.9 %shard_map.103 = (bf16[128,2048]{1,0:T(8,128)(2,1)}, bf16[128,2048]{1,0:T(8,128)(2,1)}, f32[128,1408]{1,0:T(8,128)}) custom-call(bf16[128,2048]{1,0:T(8,128)(2,1)} %get-tuple-element.4.fwd_ref, bf16[128,2048]{1,0:T(8,128)(2,1)} %get-tuple-element.3.back_ref, bf16[128,2048]{1,0:T(8,128)(2,1)} %grad_ref.1, bf16[128,2048]{1,0:T(8,128)(2,1)} %tokens_ref.1, ...), custom_call_target="tpu_custom_call" | custom-call | tf_op jit(solution)/shard_map/pallas_call | solution.py:400
  139.1 0.0 copy-start.3
  139.1 1.9 %copy.17 = bf16[128,2048]{1,0:T(8,128)(2,1)} copy(bf16[128,2048]{1,0:T(8,128)(2,1)} %get-tuple-element.10) | data formatting | bytes 1048576
  141.0 0.0 copy-done.3
  141.0 0.0 copy-start.2
  141.1 0.8 copy.18
  141.8 0.5 copy-done.2
  142.3 0.9 copy.19
  (1 shorter events, 0.0 us)
Async XLA Ops:
  0.6 1.3 copy-start
  1.9 1.0 copy-start.4
  2.9 1.0 copy-start.5
  3.9 1.0 copy-start.6
  4.8 1.1 copy-start.1
  4.9 1.0 copy-start.7
  139.1 2.0 %copy-start.3 = (bf16[128,2048]{1,0:T(8,128)(2,1)S(1)}, bf16[128,2048]{1,0:T(8,128)(2,1)}, u32[]{:S(2)}) copy-start(bf16[128,2048]{1,0:T(8,128)(2,1)} %get-tuple-element.11) | copy-start | bytes 1572868
  141.0 1.3 copy-start.2

commit v2 on v1

--- a/solution.py
+++ b/solution.py
@@ -81,9 +81,9 @@
     planes, plane, fwd_ref, back_ref, grad_ref, tokens_ref, gain_ref, gate_ref, up_ref, down_ref, sum_ref,
     fwd_out, back_out, sum_out,
     toks, weights, fwd_gate, fwd_up, back_gate, back_up, hidden, gate_diff, up_diff,
-    part, crossed, joined, gathered, grad_send, grad_recv, grad_cols,
+    part, crossed, joined, gathered, grad_send, lifted, dropped, grad_recv, grad_cols,
     stage_sem, weight_sem, up_sem, down_sem, tok_send, tok_recv, relay_send, relay_recv,
-    grad_send_sem, grad_recv_sem, cross_sem, join_send, join_recv, last_sem,
+    lift_send, lift_recv, drop_send, drop_recv, turn_send, turn_recv, cross_sem, join_send, join_recv, last_sem,
 ):
     n_fs = planes * plane
     fs, core = lax.axis_index("fs"), lax.axis_index("tp")
@@ -201,22 +201,17 @@
         def _(h):
             out[h] = wide_dot(toks[a, h], weights[w])
 
-    for wave in range(planes):
+    for d in range(planes - 1):
         for w in range(3):
-            d = wave - w
-            if 0 <= d < planes:
-                group(w, d)
-    relays(0)
-    relays(1)
-    relays_in(0)
+            group(w, d)
+    for a in range(3):
+        relays(a)
+    for a in range(3):
+        relays_in(a)
+    group(0, planes - 1)
     project(0, 0, back_gate)
-    relays_in(1)
     project(1, 0, fwd_gate)
-    relays(2)
-    for w in range(1, 3):
-        if 0 <= planes - w < planes:
-            group(w, planes - w)
-    relays_in(2)
+    group(1, planes - 1)
     project(0, 1, back_up)
     project(1, 1, fwd_up)
 
@@ -234,8 +229,7 @@
             back_gate[h, at, :] = gate * s
             back_up[h, at, :] = back_up[h, at, :] * s * (1.0 + gate * (1.0 - s))
 
-    for w in range(2, 3):
-        group(w, planes - 1)
+    group(2, planes - 1)
 
     @pl.loop(0, 2)
     def _(h):
@@ -244,28 +238,50 @@
         gate_diff[pl.ds(pl.multiple_of(h * slab, slab), slab), :] = (back * back_up[h]).astype(jnp.bfloat16)
         up_diff[pl.ds(pl.multiple_of(h * slab, slab), slab), :] = (back * back_gate[h]).astype(jnp.bfloat16)
 
-    def grad_copy(step):
-        to = (fs + step) % n_fs
-        return remote(grad_send.at[to], grad_recv.at[fs], grad_send_sem.at[to], grad_recv_sem.at[fs], (to, core))
+    def grad_hop(b, way):
+        sends, recvs, lands = (lift_send, lift_recv, lifted) if way > 0 else (drop_send, drop_recv, dropped)
+        to = (fs + way * plane + n_fs) % n_fs
+        return remote(grad_send.at[b], lands.at[b], sends.at[b], recvs.at[b], (to, core))
 
     diff_turned = gate_diff[...].T
 
     for step in range(planes):
-        there = (level + step + 1) % planes
+        there = jnp.where(2 * level < planes, planes - 1 - step, step)
         cols = pl.ds(pl.multiple_of(there * plane * depth, plane * depth), plane * depth)
         product = jnp.dot(diff_turned[:, :slab], toks[0, 0, :, cols], preferred_element_type=jnp.float32)
         product = product + jnp.dot(diff_turned[:, slab:], toks[0, 1, :, cols], preferred_element_type=jnp.float32)
         product = product.astype(jnp.bfloat16)
         for q in range(plane):
             grad_send[there * plane + q] = product[:, q * depth : (q + 1) * depth]
-        for q in range(plane):
-            to = there * plane + q
-
-            @pl.when(to != fs)
+        for way, first in ((1, 0), (-1, planes - 1)):
+
+            @pl.when(jnp.logical_and(level == first, there != first))
             def _():
-                remote(grad_send.at[to], grad_recv.at[fs], grad_send_sem.at[to], grad_recv_sem.at[fs], (to, core)).start()
-
-    grad_recv[fs] = grad_send[fs]
+                for q in range(plane):
+                    grad_hop(there * plane + q, way).start()
+
+    def serve(i):
+        for way in (1, -1):
+            lands = lifted if way > 0 else dropped
+            there = planes - 1 - i if way > 0 else i
+            left = (there - level) * way
+
+            @pl.when(jnp.logical_and(can[-way], left >= 0))
+            def _():
+                @pl.loop(0, plane)
+                def _(q):
+                    b = there * plane + q
+                    grad_hop(b, way).wait_recv()
+                    total = grad_send[b].astype(jnp.float32) + lands[b].astype(jnp.float32)
+                    grad_send[b] = total.astype(jnp.bfloat16)
+
+                    @pl.when(left > 0)
+                    def _():
+                        grad_hop(b, way).start()
+
+    def turn(step):
+        q = (place + step) % plane
+        return remote(grad_send.at[level * plane + q], grad_recv.at[place], turn_send.at[step], turn_recv.at[place], (level * plane + q, core))
 
     def cross(k):
         return remote(part.at[k, 1 - core], crossed.at[k], cross_sem.at[k, 0], cross_sem.at[k, 1], sibling)
@@ -303,6 +319,11 @@
             joined[k, q] = total.astype(jnp.bfloat16)
             if step < plane - 1:
                 join(k, step + 1).start()
+    for i in range(planes):
+        serve(i)
+    for step in range(1, plane):
+        turn(step).start()
+    grad_recv[place] = grad_send[fs]
     for k in range(2):
         gathered[k, place] = joined[k, place]
 
@@ -342,14 +363,11 @@
     for k in range(2):
         last(k).start()
 
-    for step in range(1, n_fs):
-        src = (fs + step) % n_fs
-        remote(grad_send.at[src], grad_recv.at[src], grad_send_sem.at[src], grad_recv_sem.at[src], sibling).wait_recv()
+    for step in range(1, plane):
+        q = (place + step) % plane
+        remote(grad_send.at[fs], grad_recv.at[q], turn_send.at[0], turn_recv.at[q], sibling).wait_recv()
     for q in range(plane):
-        total = grad_recv[q].astype(jnp.float32)
-        for z in range(1, planes):
-            total = total + grad_recv[z * plane + q].astype(jnp.float32)
-        grad_cols[q * rows : (q + 1) * rows, :] = total
+        grad_cols[q * rows : (q + 1) * rows, :] = grad_recv[q].astype(jnp.float32)
 
     @pl.loop(0, grad_cols.shape[0] // 128)
     def _(t):
@@ -374,8 +392,20 @@
         for step in range(1, plane):
             tok_copy(a, step).wait_send()
             relay(a, (place + step) % plane).wait_send()
-    for step in range(1, n_fs):
-        grad_copy(step).wait_send()
+    for step in range(1, plane):
+        turn(step).wait_send()
+    for way in (1, -1):
+
+        @pl.when(can[way])
+        def _():
+            @pl.loop(0, planes)
+            def _(there):
+                @pl.when((there - level) * way > 0)
+                def _():
+                    @pl.loop(0, plane)
+                    def _(q):
+                        grad_hop(there * plane + q, way).wait_send()
+
     for k in range(2):
         cross(k).wait_send()
         for step in range(1, plane):
@@ -422,6 +452,8 @@
             pltpu.VMEM((2, plane, half, width), narrow),
             pltpu.VMEM((n_fs, rows, depth), narrow),
             pltpu.VMEM((n_fs, rows, depth), narrow),
+            pltpu.VMEM((n_fs, rows, depth), narrow),
+            pltpu.VMEM((plane, rows, depth), narrow),
             pltpu.VMEM((cols, depth), full),
             dma((3, plane)),
             dma((3, n_fs)),
@@ -433,6 +465,10 @@
             dma((3, plane)),
             dma((n_fs,)),
             dma((n_fs,)),
+            dma((n_fs,)),
+            dma((n_fs,)),
+            dma((plane,)),
+            dma((plane,)),
             dma((2, 2)),
             dma((2, plane)),
             dma((2, plane)),

time: 144 us -> 135 us (0.938)
  the two profiles are of different devices: /device:TPU:0 before, /device:TPU:10 now
where the time goes in v2:
time: 135 us
  Pallas kernels  123 us (91%)
  local copies, waits for them, and re-layouts  7.84 us (6%)
  other arithmetic  2.75 us (2%)
    pallas_call x1, Pallas kernels, fused_shards(): pl.pallas_call(functools.partial(layer_kernel, planes, plane), out_shape=...  123 us
    unnamed x22, local copies, waits for them, and re-layouts  7.84 us

profile of v2, /device:TPU:10, one launch (start us, length us, event | category | flops | bytes accessed | tf_op | source)
XLA Modules:
  0.0 134.6 jit_solution(11557813569391576412)
XLA Ops:
  0.6 0.0 copy-start
  0.6 1.3 fusion
  1.9 0.0 copy-done
  1.9 0.0 copy-start.4
  1.9 0.2 fusion.3
  2.1 0.8 copy-done.4
  2.9 0.0 copy-start.5
  2.9 0.9 copy.11
  3.8 0.1 copy-done.5
  3.9 0.0 copy-start.6
  3.9 0.9 copy.12
  4.8 0.0 copy-start.1
  4.8 0.1 copy-done.6
  4.9 0.0 copy-start.7
  4.9 0.9 copy.13
  5.8 0.1 copy-done.1
  5.9 0.0 copy-done.7
  5.9 1.3 fusion.5
  7.1 123.4 %shard_map.103 = (bf16[128,2048]{1,0:T(8,128)(2,1)}, bf16[128,2048]{1,0:T(8,128)(2,1)}, f32[128,1408]{1,0:T(8,128)}) custom-call(bf16[128,2048]{1,0:T(8,128)(2,1)} %get-tuple-element.4.fwd_ref, bf16[128,2048]{1,0:T(8,128)(2,1)} %get-tuple-element.3.back_ref, bf16[128,2048]{1,0:T(8,128)(2,1)} %grad_ref.1, bf16[128,2048]{1,0:T(8,128)(2,1)} %tokens_ref.1, ...), custom_call_target="tpu_custom_call" | custom-call | tf_op jit(solution)/shard_map/pallas_call | solution.py:430
  130.5 0.0 copy-start.3
  130.5 1.9 %copy.17 = bf16[128,2048]{1,0:T(8,128)(2,1)} copy(bf16[128,2048]{1,0:T(8,128)(2,1)} %get-tuple-element.10) | data formatting | bytes 1048576
  132.5 0.0 copy-done.3
  132.5 0.0 copy-start.2
  132.5 0.8 copy.18
  133.3 0.5 copy-done.2
  133.8 0.9 copy.19
  (1 shorter events, 0.0 us)
Async XLA Ops:
  0.6 1.3 copy-start
  1.9 1.0 copy-start.4
  2.9 1.0 copy-start.5
  3.9 1.0 copy-start.6
  4.8 1.1 copy-start.1
  4.9 1.0 copy-start.7
  130.5 2.0 %copy-start.3 = (bf16[128,2048]{1,0:T(8,128)(2,1)S(1)}, bf16[128,2048]{1,0:T(8,128)(2,1)}, u32[]{:S(2)}) copy-start(bf16[128,2048]{1,0:T(8,128)(2,1)} %get-tuple-element.11) | copy-start | bytes 1572868
  132.5 1.3 copy-start.2

commit v3 on v2

--- a/solution.py
+++ b/solution.py
@@ -78,9 +78,9 @@
 
 
 def layer_kernel(
-    planes, plane, fwd_ref, back_ref, grad_ref, tokens_ref, gain_ref, gate_ref, up_ref, down_ref, sum_ref,
+    planes, plane, fwd_ref, tokens_ref, grad_ref, gain_ref, gate_ref, up_ref, down_ref, sum_ref,
     fwd_out, back_out, sum_out,
-    toks, weights, fwd_gate, fwd_up, back_gate, back_up, hidden, gate_diff, up_diff,
+    turned, normed, toks, weights, fwd_gate, fwd_up, back_gate, back_up, hidden, gate_diff, up_diff,
     part, crossed, joined, gathered, grad_send, lifted, dropped, grad_recv, grad_cols,
     stage_sem, weight_sem, up_sem, down_sem, tok_send, tok_recv, relay_send, relay_recv,
     lift_send, lift_recv, drop_send, drop_recv, turn_send, turn_recv, cross_sem, join_send, join_recv, last_sem,
@@ -90,7 +90,7 @@
     level, place = fs // plane, fs % plane
     sibling = (fs, 1 - core)
     rows = weights.shape[1]
-    depth = gate_ref.shape[1]
+    depth = gate_ref.shape[0]
     half = fwd_ref.shape[0] // 2
     slab = half * plane
     width = fwd_ref.shape[1]
@@ -99,6 +99,20 @@
     for step in range(1, n_fs):
         pl.semaphore_signal(barrier, inc=1, device_id=((fs + step) % n_fs, core), device_id_type=MESH)
     pl.semaphore_signal(barrier, inc=1, device_id=sibling, device_id_type=MESH)
+
+    @pl.loop(0, turned.shape[1] // 128)
+    def _(t):
+        at = pl.ds(pl.multiple_of(t * 128, 128), 128)
+        turned[0, at, :] = gate_ref[:, at].T
+        turned[1, at, :] = up_ref[:, at].T
+        turned[2, at, :] = down_ref[:, at].T
+
+    @pl.loop(0, fwd_ref.shape[0] // 16)
+    def _(r):
+        at = pl.ds(pl.multiple_of(r * 16, 16), 16)
+        for a, ref in ((0, tokens_ref), (1, fwd_ref)):
+            normed[a, at, :] = normalize(ref[at, :], gain_ref[...])[2]
+
     pl.semaphore_wait(barrier, n_fs)
 
     def remote(src, dst, send, recv, device):
@@ -106,10 +120,8 @@
             src_ref=src, dst_ref=dst, send_sem=send, recv_sem=recv, device_id=device, device_id_type=MESH
         )
 
-    own = (gate_ref, up_ref, down_ref)
-
     def own_block(w, q):
-        return own[w].at[pl.ds(pl.multiple_of(q * rows, rows), rows), :]
+        return turned.at[w, pl.ds(pl.multiple_of(q * rows, rows), rows), :]
 
     def block(w, src):
         return weights.at[w, :, pl.ds(pl.multiple_of(src * depth, depth), depth)]
@@ -132,7 +144,8 @@
         def _():
             hop(w, src, source, step).start()
 
-    token_refs = (back_ref, fwd_ref, grad_ref)
+    def token_rows(a, at):
+        return grad_ref.at[at, :] if a == 2 else normed.at[a, at, :]
 
     def tok_block(a, h, q):
         return toks.at[a, h, pl.ds(pl.multiple_of(q * half, half), half), :]
@@ -140,7 +153,7 @@
     def tok_copy(a, step):
         q = (place + step) % plane
         return remote(
-            token_refs[a].at[pl.ds(pl.multiple_of(core * half, half), half), :],
+            token_rows(a, pl.ds(pl.multiple_of(core * half, half), half)),
             tok_block(a, core, place), tok_send.at[a, step], tok_recv.at[a, place], (level * plane + q, core),
         )
 
@@ -162,10 +175,10 @@
         for step in range(1, plane):
             tok_copy(a, step).start()
     for w in range(3):
-        weights[w, :, pl.ds(pl.multiple_of(fs * depth, depth), depth)] = own[w][pl.ds(pl.multiple_of(place * rows, rows), rows), :]
+        weights[w, :, pl.ds(pl.multiple_of(fs * depth, depth), depth)] = turned[w, pl.ds(pl.multiple_of(place * rows, rows), rows), :]
     for a in range(3):
         for h in range(2):
-            toks[a, h, pl.ds(pl.multiple_of(place * half, half), half), :] = token_refs[a][pl.ds(h * half, half), :]
+            toks[a, h, pl.ds(pl.multiple_of(place * half, half), half), :] = token_rows(a, pl.ds(h * half, half))[...]
 
     def group(w, d):
         if d == 0:
@@ -422,8 +435,6 @@
     half = tokens // 2
     slab = half * plane
     n_fs = planes * plane
-    fwd_normed = normalize(fwd_tokens, norm_gain)[2]
-    back_normed = normalize(back_tokens, norm_gain)[2]
     narrow, full = jnp.bfloat16, jnp.float32
     dma = pltpu.SemaphoreType.DMA
     vmem = pl.BlockSpec(memory_space=pltpu.VMEM)
@@ -434,9 +445,11 @@
             jax.ShapeDtypeStruct((tokens, width), narrow),
             jax.ShapeDtypeStruct((depth, cols), full),
         ),
-        in_specs=[vmem] * 9,
+        in_specs=[vmem] * 8,
         out_specs=(vmem,) * 3,
         scratch_shapes=[
+            pltpu.VMEM((3, cols, depth), narrow),
+            pltpu.VMEM((2, tokens, width), narrow),
             pltpu.VMEM((3, 2, slab, width), narrow),
             pltpu.VMEM((3, rows, width), narrow),
             pltpu.VMEM((2, slab, rows), full),
@@ -478,8 +491,8 @@
             collective_id=0, has_side_effects=True, vmem_limit_bytes=56 * 2**20
         ),
     )(
-        fwd_normed, back_normed, out_grad, back_tokens, norm_gain.reshape(1, width),
-        gate_weight.T, up_weight.T, down_weight.T, gate_grad_sum,
+        fwd_tokens, back_tokens, out_grad, norm_gain.reshape(1, width),
+        gate_weight, up_weight, down_weight, gate_grad_sum,
     )
 
 

time: 135 us -> 128 us (0.948)
  local copies, waits for them, and re-layouts: 7.84 us -> 4.1 us
  other arithmetic: 2.75 us -> 0 us
    unnamed x22 -> x7, local copies, waits for them, and re-layouts: 7.84 us -> 4.1 us
    reduce_sum x2 -> x0, other arithmetic: 1.47 us -> none  [normalize(): jnp.mean(values * values, axis=-1, keepdims=True) + norm_eps]
where the time goes in v3:
time: 128 us
  Pallas kernels  123 us (96%)
  local copies, waits for them, and re-layouts  4.1 us (3%)
    pallas_call x1, Pallas kernels, fused_shards(): pl.pallas_call(functools.partial(layer_kernel, planes, plane), out_shape=...  123 us
    unnamed x7, local copies, waits for them, and re-layouts  4.1 us

profile of v3, /device:TPU:10, one launch (start us, length us, event | category | flops | bytes accessed | tf_op | source)
XLA Modules:
  0.0 128.0 jit_solution(15269163737693887512)
XLA Ops:
  0.6 123.2 %shard_map.103 = (bf16[128,2048]{1,0:T(8,128)(2,1)}, bf16[128,2048]{1,0:T(8,128)(2,1)}, f32[128,1408]{1,0:T(8,128)}) custom-call(bf16[128,2048]{1,0:T(8,128)(2,1)} %fwd_ref.1, bf16[128,2048]{1,0:T(8,128)(2,1)} %tokens_ref.1, bf16[128,2048]{1,0:T(8,128)(2,1)} %grad_ref.1, f32[1,2048]{1,0:T(1,128)} %bitcast.1, bf16[128,1408]{1,0:T(8,128)(2,1)} %gate_ref.1, ...), custom_call_target="tpu_custom_call" | custom-call | tf_op jit(solution)/shard_map/pallas_call | solution.py:441
  123.9 0.0 copy-start.1
  123.9 1.9 %copy.14 = bf16[128,2048]{1,0:T(8,128)(2,1)} copy(bf16[128,2048]{1,0:T(8,128)(2,1)} %get-tuple-element.6) | data formatting | bytes 1048576
  125.8 0.0 copy-done.1
  125.8 0.0 copy-start
  125.8 0.8 copy.15
  126.6 0.5 copy-done
  127.1 0.9 copy.16
Async XLA Ops:
  123.9 2.0 %copy-start.1 = (bf16[128,2048]{1,0:T(8,128)(2,1)S(1)}, bf16[128,2048]{1,0:T(8,128)(2,1)}, u32[]{:S(2)}) copy-start(bf16[128,2048]{1,0:T(8,128)(2,1)} %get-tuple-element.7) | copy-start | bytes 1572868
  125.8 1.3 %copy-start = (f32[128,1408]{1,0:T(8,128)S(1)}, f32[128,1408]{1,0:T(8,128)}, u32[]{:S(2)}) copy-start(f32[128,1408]{1,0:T(8,128)} %get-tuple-element.8) | copy-start | bytes 2162692

commit v4 on v3

--- a/solution.py
+++ b/solution.py
@@ -96,8 +96,12 @@
     width = fwd_ref.shape[1]
 
     barrier = pltpu.get_barrier_semaphore()
-    for step in range(1, n_fs):
-        pl.semaphore_signal(barrier, inc=1, device_id=((fs + step) % n_fs, core), device_id_type=MESH)
+    for step in range(1, plane):
+        to = level * plane + (place + step) % plane
+        pl.semaphore_signal(barrier, inc=1, device_id=(to, core), device_id_type=MESH)
+    for step in (1, planes - 1):
+        to = (fs + step * plane) % n_fs
+        pl.semaphore_signal(barrier, inc=1, device_id=(to, core), device_id_type=MESH)
     pl.semaphore_signal(barrier, inc=1, device_id=sibling, device_id_type=MESH)
 
     @pl.loop(0, turned.shape[1] // 128)
@@ -113,7 +117,7 @@
         for a, ref in ((0, tokens_ref), (1, fwd_ref)):
             normed[a, at, :] = normalize(ref[at, :], gain_ref[...])[2]
 
-    pl.semaphore_wait(barrier, n_fs)
+    pl.semaphore_wait(barrier, plane + 2)
 
     def remote(src, dst, send, recv, device):
         return pltpu.make_async_remote_copy(

time: 128 us -> 126 us (0.984)
  Pallas kernels: 123 us -> 121 us
    pallas_call x1, Pallas kernels: 123 us -> 121 us  [fused_shards(): pl.pallas_call(functools.partial(layer_kernel, planes, plane), out_shape=...]
where the time goes in v4:
time: 126 us
  Pallas kernels  121 us (96%)
  local copies, waits for them, and re-layouts  4.1 us (3%)
    pallas_call x1, Pallas kernels, fused_shards(): pl.pallas_call(functools.partial(layer_kernel, planes, plane), out_shape=...  121 us
    unnamed x7, local copies, waits for them, and re-layouts  4.1 us

profile of v4, /device:TPU:10, one launch (start us, length us, event | category | flops | bytes accessed | tf_op | source)
XLA Modules:
  0.0 126.1 jit_solution(12393041260954732137)
XLA Ops:
  0.6 121.4 %shard_map.103 = (bf16[128,2048]{1,0:T(8,128)(2,1)}, bf16[128,2048]{1,0:T(8,128)(2,1)}, f32[128,1408]{1,0:T(8,128)}) custom-call(bf16[128,2048]{1,0:T(8,128)(2,1)} %fwd_ref.1, bf16[128,2048]{1,0:T(8,128)(2,1)} %tokens_ref.1, bf16[128,2048]{1,0:T(8,128)(2,1)} %grad_ref.1, f32[1,2048]{1,0:T(1,128)} %bitcast.1, bf16[128,1408]{1,0:T(8,128)(2,1)} %gate_ref.1, ...), custom_call_target="tpu_custom_call" | custom-call | tf_op jit(solution)/shard_map/pallas_call | solution.py:445
  122.0 0.0 copy-start.1
  122.0 1.9 %copy.14 = bf16[128,2048]{1,0:T(8,128)(2,1)} copy(bf16[128,2048]{1,0:T(8,128)(2,1)} %get-tuple-element.6) | data formatting | bytes 1048576
  124.0 0.0 copy-done.1
  124.0 0.0 copy-start
  124.0 0.8 copy.15
  124.8 0.5 copy-done
  125.3 0.9 copy.16
Async XLA Ops:
  122.0 2.0 %copy-start.1 = (bf16[128,2048]{1,0:T(8,128)(2,1)S(1)}, bf16[128,2048]{1,0:T(8,128)(2,1)}, u32[]{:S(2)}) copy-start(bf16[128,2048]{1,0:T(8,128)(2,1)} %get-tuple-element.7) | copy-start | bytes 1572868
  124.0 1.3 %copy-start = (f32[128,1408]{1,0:T(8,128)S(1)}, f32[128,1408]{1,0:T(8,128)}, u32[]{:S(2)}) copy-start(f32[128,1408]{1,0:T(8,128)} %get-tuple-element.8) | copy-start | bytes 2162692
